TPU v7x, 32 devices: a whole 2x2x4 slice. The times are simulated.
32 devices in a mesh: sp: 8 (over z, y), tp: 4 (over x, core).
Axes of the slice: x: 2, y: 2, z: 4, core: 2. Of those that a mesh axis runs over, the one named last changes fastest.
Arguments:
- stream: bfloat16 [1024, 2048], P('sp'), may hold values from -12 to 12
- out_grad: bfloat16 [1024, 2048], P('sp'), may hold values from -6 to 6
- routes: int32 [1024, 2], P('sp'), may hold values from 0 to 7, all different within a row; in each aligned block of 128 rows (0 to 127, 128 to 255, ...) at most 64 rows name the same one
- route_weight: float32 [1024, 2], P('sp'), may hold values from 0.2 to 1
- queries: bfloat16 [1024, 8, 128], P('sp', 'tp'), may hold values from -6 to 6
- key_vectors: bfloat16 [1024, 8, 128], P('sp', 'tp'), may hold values from -6 to 6
- value_vectors: bfloat16 [1024, 8, 256], P('sp', 'tp'), may hold values from -6 to 6
- log_decay: float32 [1024, 8], P('sp', 'tp'), may hold values from -1 to 0
- out_proj: bfloat16 [2048, 2048], P(None, 'tp'), may hold values from -0.125 to 0.125
- gate_weight: bfloat16 [8, 2048, 1024], P('sp', None, 'tp'), may hold values from -0.125 to 0.125
- up_weight: bfloat16 [8, 2048, 1024], P('sp', None, 'tp'), may hold values from -0.125 to 0.125
- down_weight: bfloat16 [8, 1024, 2048], P('sp', 'tp'), may hold values from -0.1875 to 0.1875
Outputs:
- gate_grad: bfloat16 [8, 2048, 1024], P('sp', None, 'tp')
- up_grad: bfloat16 [8, 2048, 1024], P('sp', None, 'tp')
- down_grad: bfloat16 [8, 1024, 2048], P('sp', 'tp')
- proj_grad: float32 [2048, 2048], P('sp', 'tp')
- query_grad: bfloat16 [1024, 8, 128], P('sp', 'tp')
- key_grad: bfloat16 [1024, 8, 128], P('sp', 'tp')
- value_grad: bfloat16 [1024, 8, 256], P('sp', 'tp')
Inputs may be any that keep to these rules, and one draw needn't show every extreme that they name: `routes`: each row names two different experts. In each aligned block of 128 rows no expert is named by more than 64 rows, and in some block an expert is named by exactly 64.
All inputs are finite; a program needn't handle non-finite values.
Results may differ from a plain program's by a relative error of at most 0.025.
Values may be sent and summed in bfloat16 or wider, within the bound.
A program may use at most 128 MiB of HBM per device.

v0:
```python
import jax
import jax.numpy as jnp
from jax import lax
from jax.sharding import PartitionSpec as P

CLAMP_LIMIT = 7.0
GATE_SLOPE = 1.702
EPSILON = 1e-06
TOP_PRECISION = lax.Precision.HIGHEST


def prefix(x, axis, join, neutral):
    place = lax.axis_index(axis)
    gathered = jax.tree.map(
        lambda a, kind: lax.all_gather(a.astype(kind), axis), x, (jnp.bfloat16, jnp.bfloat16)
    )
    state = jax.tree.map(lambda a, e: jnp.zeros_like(a) + jnp.asarray(e, a.dtype), x, neutral)

    def one(hop, state):
        return join(
            state,
            jax.tree.map(
                lambda a, own: lax.dynamic_index_in_dim(a, hop, 0, False).astype(own.dtype),
                gathered,
                x,
            ),
        )

    return lax.fori_loop(0, place, one, state)


def prefix_2(x, axis, join, neutral):
    count = lax.axis_size(axis)
    place = lax.axis_index(axis)
    ahead = count - 1 - place
    gathered = jax.tree.map(
        lambda a, kind: lax.all_gather(a.astype(kind), axis),
        x,
        jax.tree.map(lambda a: jnp.bfloat16 if a.dtype == jnp.float32 else a.dtype, x),
    )
    state = jax.tree.map(lambda a, e: jnp.zeros_like(a) + jnp.asarray(e, a.dtype), x, neutral)

    def one(hop, state):
        source = count - 1 - hop
        return join(
            state,
            jax.tree.map(
                lambda a, own: lax.dynamic_index_in_dim(a, source, 0, False).astype(own.dtype),
                gathered,
                x,
            ),
        )

    return lax.fori_loop(0, ahead, one, state)


def slot_numbers(route_block, expert_count):
    flat_ids = route_block.reshape(-1)
    onehot = (flat_ids[:, None] == jnp.arange(expert_count, dtype=jnp.int32)[None, :]).astype(
        jnp.int32
    )
    before = jnp.cumsum(onehot, axis=0) - onehot
    return (flat_ids, jnp.sum(before * onehot, axis=1))


def rotation_tables(start, count, key_width):
    frequency = 1.0 / 10000.0 ** jnp.linspace(0.0, 1.0, key_width // 2, dtype=jnp.float32)
    token_position = (start + jnp.arange(count, dtype=jnp.int32)).astype(jnp.float32)
    angles = token_position[:, None] * frequency[None, :]
    return (jnp.cos(angles), jnp.sin(angles))


def turn(field, cosines, sines):
    paired = field.reshape(field.shape[:-1] + (field.shape[-1] // 2, 2))
    even_part = paired[..., 0]
    odd_part = paired[..., 1]
    cos_rows = cosines[:, None, :]
    sin_rows = sines[:, None, :]
    turned = jnp.stack(
        [even_part * cos_rows - odd_part * sin_rows, odd_part * cos_rows + even_part * sin_rows],
        axis=-1,
    )
    return turned.reshape(field.shape)


def decay_combine(earlier, next_rows):
    return (earlier[0] * next_rows[0], next_rows[1] + next_rows[0][:, None, None] * earlier[1])


def expert_local(routed_rows, routed_grads, gate_w, up_w, down_w):
    gate_pre = jnp.dot(routed_rows, gate_w, preferred_element_type=jnp.float32)
    up_pre = jnp.dot(routed_rows, up_w, preferred_element_type=jnp.float32)
    gate_clip = jnp.minimum(gate_pre, CLAMP_LIMIT)
    up_clip = jnp.clip(up_pre, -CLAMP_LIMIT, CLAMP_LIMIT)
    sigmoid_gate = jax.nn.sigmoid(GATE_SLOPE * gate_clip)
    activated = (gate_clip * sigmoid_gate * (up_clip + 1.0)).astype(jnp.bfloat16)
    down_part = lax.dot_general(
        activated, routed_grads, (((0,), (0,)), ((), ())), preferred_element_type=jnp.float32
    )
    act_grad = lax.dot_general(
        routed_grads, down_w, (((1,), (1,)), ((), ())), preferred_element_type=jnp.float32
    )
    slope = sigmoid_gate + GATE_SLOPE * gate_clip * sigmoid_gate * (1.0 - sigmoid_gate)
    gate_pre_grad = jnp.where(
        gate_pre < CLAMP_LIMIT, act_grad * (up_clip + 1.0) * slope, 0.0
    ).astype(jnp.bfloat16)
    up_pre_grad = jnp.where(
        jnp.abs(up_pre) < CLAMP_LIMIT, act_grad * gate_clip * sigmoid_gate, 0.0
    ).astype(jnp.bfloat16)
    gate_part = lax.dot_general(
        routed_rows, gate_pre_grad, (((0,), (0,)), ((), ())), preferred_element_type=jnp.float32
    )
    up_part = lax.dot_general(
        routed_rows, up_pre_grad, (((0,), (0,)), ((), ())), preferred_element_type=jnp.float32
    )
    back_rows = lax.dot_general(
        gate_pre_grad, gate_w, (((1,), (1,)), ((), ())), preferred_element_type=jnp.float32
    )
    back_rows = back_rows + lax.dot_general(
        up_pre_grad, up_w, (((1,), (1,)), ((), ())), preferred_element_type=jnp.float32
    )
    return (
        gate_part.astype(jnp.bfloat16),
        up_part.astype(jnp.bfloat16),
        down_part.astype(jnp.bfloat16),
        back_rows.astype(jnp.bfloat16),
    )


def per_device(
    stream,
    out_grad,
    routes,
    route_weight,
    queries,
    key_vectors,
    value_vectors,
    log_decay,
    out_proj,
    gate_weight,
    up_weight,
    down_weight,
):
    experts = lax.axis_size("sp")
    tokens_here = stream.shape[0]
    model_width = stream.shape[1]
    capacity = 4 * tokens_here // experts
    pair_count = 2 * tokens_here
    flat_ids, slot_ids = slot_numbers(routes, experts)
    destination = flat_ids * capacity + slot_ids
    source = (
        jnp.full((experts * capacity,), -1, jnp.int32)
        .at[destination]
        .set(jnp.arange(pair_count, dtype=jnp.int32))
    )
    present = (source >= 0)[:, None]
    picked = jnp.maximum(source, 0)
    zero_value = jnp.zeros((), jnp.bfloat16)
    pair_grad = (route_weight[:, :, None] * out_grad[:, None, :].astype(jnp.float32)).astype(
        jnp.bfloat16
    )
    pair_grad = pair_grad.reshape(pair_count, model_width)
    send_rows = jnp.where(present, jnp.take(stream, picked // 2, axis=0), zero_value)
    send_rows = send_rows.reshape(experts, capacity, model_width)
    send_grads = jnp.where(present, jnp.take(pair_grad, picked, axis=0), zero_value)
    send_grads = send_grads.reshape(experts, capacity, model_width)
    quarter = model_width // lax.axis_size("tp")
    col_start = lax.axis_index("tp") * quarter
    quarters = (
        lax.dynamic_slice_in_dim(send_rows, col_start, quarter, 2),
        lax.dynamic_slice_in_dim(send_grads, col_start, quarter, 2),
    )
    quarters = (
        lax.all_to_all(quarters[0], "sp", split_axis=0, concat_axis=0, tiled=True),
        lax.all_to_all(quarters[1], "sp", split_axis=0, concat_axis=0, tiled=True),
    )
    routed_rows, routed_grads = (
        lax.all_gather(quarters[0], "tp", axis=2, tiled=True),
        lax.all_gather(quarters[1], "tp", axis=2, tiled=True),
    )
    routed_rows = routed_rows.reshape(experts * capacity, model_width)
    routed_grads = routed_grads.reshape(experts * capacity, model_width)
    gate_part, up_part, down_part, back_rows = expert_local(
        routed_rows, routed_grads, gate_weight[0], up_weight[0], down_weight[0]
    )
    summed = lax.psum(back_rows, "tp").astype(jnp.float32).astype(jnp.bfloat16)
    returned = lax.all_to_all(
        summed.reshape(experts, capacity, model_width),
        "sp",
        split_axis=0,
        concat_axis=0,
        tiled=True,
    )
    returned = returned.reshape(experts * capacity, model_width)
    per_pair = (
        jnp.take(returned, destination, axis=0)
        .reshape(tokens_here, 2, model_width)
        .astype(jnp.float32)
    )
    resid_grad = (out_grad.astype(jnp.float32) + per_pair[:, 0] + per_pair[:, 1]).astype(
        jnp.bfloat16
    )
    heads_local = queries.shape[1]
    key_width = queries.shape[2]
    value_width = value_vectors.shape[2]
    key_scale = key_width ** (-0.5)
    cosines, sines = rotation_tables(lax.axis_index("sp") * tokens_here, tokens_here, key_width)
    query_rotated = turn(queries.astype(jnp.float32), cosines, sines).transpose(1, 0, 2)
    key_rotated = (turn(key_vectors.astype(jnp.float32), cosines, sines) * key_scale).transpose(
        1, 0, 2
    )
    value_per_head = value_vectors.astype(jnp.float32).transpose(1, 0, 2)
    running_total = jnp.cumsum(log_decay, axis=0).T
    block_total = running_total[:, -1]
    causal = (jnp.arange(tokens_here)[:, None] >= jnp.arange(tokens_here)[None, :])[None]
    difference = running_total[:, :, None] - running_total[:, None, :]
    decay_mask = jnp.where(causal, jnp.exp(jnp.where(causal, difference, 0.0)), 0.0)
    per_head_decay = jnp.exp(running_total)
    remaining_decay = jnp.exp(block_total[:, None] - running_total)
    carried = jnp.exp(block_total)
    inner_state = jnp.einsum(
        "wfs,wfi->wsi",
        key_rotated * remaining_decay[..., None],
        value_per_head,
        precision=TOP_PRECISION,
    )
    identity = (jnp.ones_like(carried), jnp.zeros_like(inner_state))
    incoming_state = prefix((carried, inner_state), "sp", decay_combine, identity)[1]
    weights = (
        jnp.einsum("hik,hjk->hij", query_rotated, key_rotated, precision=TOP_PRECISION) * decay_mask
    )
    retained_output = jnp.einsum("hij,hjv->hiv", weights, value_per_head, precision=TOP_PRECISION)
    retained_output = retained_output + per_head_decay[..., None] * jnp.einsum(
        "dzr,drs->dzs", query_rotated, incoming_state, precision=TOP_PRECISION
    )
    inverse_rms = lax.rsqrt(
        jnp.mean(retained_output * retained_output, axis=-1, keepdims=True) + EPSILON
    )
    normed = retained_output * inverse_rms
    normed_bf = (
        normed.transpose(1, 0, 2)
        .reshape(tokens_here, heads_local * value_width)
        .astype(jnp.bfloat16)
    )
    proj_grad = lax.psum_scatter(
        lax.dot_general(
            resid_grad, normed_bf, (((0,), (0,)), ((), ())), preferred_element_type=jnp.float32
        ),
        "sp",
        scatter_dimension=0,
        tiled=True,
    )
    normed_grad = jnp.dot(resid_grad, out_proj, preferred_element_type=jnp.float32)
    normed_grad = normed_grad.reshape(tokens_here, heads_local, value_width).transpose(1, 0, 2)
    retention_gradient = inverse_rms * (
        normed_grad - normed * jnp.mean(normed_grad * normed, axis=-1, keepdims=True)
    )
    inner_gradient = jnp.einsum(
        "gwn,gwj->gnj",
        query_rotated * per_head_decay[..., None],
        retention_gradient,
        precision=TOP_PRECISION,
    )
    future_gradient = prefix_2((carried, inner_gradient), "sp", decay_combine, identity)[1]
    score_grad = (
        jnp.einsum("hiv,hjv->hij", retention_gradient, value_per_head, precision=TOP_PRECISION)
        * decay_mask
    )
    query_portion = jnp.einsum("hij,hjk->hik", score_grad, key_rotated, precision=TOP_PRECISION)
    query_portion = query_portion + per_head_decay[..., None] * jnp.einsum(
        "bpl,btl->bpt", retention_gradient, incoming_state, precision=TOP_PRECISION
    )
    key_portion = jnp.einsum("hij,hik->hjk", score_grad, query_rotated, precision=TOP_PRECISION)
    key_portion = key_portion + remaining_decay[..., None] * jnp.einsum(
        "uxn,ubn->uxb", value_per_head, future_gradient, precision=TOP_PRECISION
    )
    value_portion = jnp.einsum("hij,hiv->hjv", weights, retention_gradient, precision=TOP_PRECISION)
    value_portion = value_portion + remaining_decay[..., None] * jnp.einsum(
        "bui,bim->bum", key_rotated, future_gradient, precision=TOP_PRECISION
    )
    query_grad = turn(query_portion.transpose(1, 0, 2), cosines, -sines).astype(jnp.bfloat16)
    key_grad = (turn(key_portion.transpose(1, 0, 2), cosines, -sines) * key_scale).astype(
        jnp.bfloat16
    )
    value_grad = value_portion.transpose(1, 0, 2).astype(jnp.bfloat16)
    return (
        gate_part[None],
        up_part[None],
        down_part[None],
        proj_grad,
        query_grad,
        key_grad,
        value_grad,
    )


def solution(mesh):
    in_specs = (
        P("sp", None),
        P("sp", None),
        P("sp", None),
        P("sp", None),
        P("sp", "tp", None),
        P("sp", "tp", None),
        P("sp", "tp", None),
        P("sp", "tp"),
        P(None, "tp"),
        P("sp", None, "tp"),
        P("sp", None, "tp"),
        P("sp", "tp", None),
    )
    out_specs = (
        P("sp", None, "tp"),
        P("sp", None, "tp"),
        P("sp", "tp", None),
        P("sp", "tp"),
        P("sp", "tp", None),
        P("sp", "tp", None),
        P("sp", "tp", None),
    )
    return jax.shard_map(
        per_device, mesh=mesh, in_specs=in_specs, out_specs=out_specs, check_vma=False
    )
```

profile of v0, /device:TPU:0, one launch (start us, length us, event | category | flops | bytes accessed | tf_op | source)
XLA Modules:
  0.0 386.7 jit_solution(6628498509636234050)
XLA Ops:
  8.1 0.8 broadcast_multiply_fusion.1
  11.2 1.4 scatter_custom_fusion
  12.6 3.5 mul.382
  16.1 3.7 mul.383
  20.3 2.7 multiply_convert_fusion
  23.0 6.6 %gather_fusion.1 = bf16[512,2048]{1,0:T(8,128)(2,1)} fusion(bf16[256,2048]{1,0:T(8,128)(2,1)} %multiply_convert_fusion, s32[1024]{0:T(1024)S(1)} %pad_clamp_fusion.1), kind=kCustom, calls=%fused_computation.1 | custom fusion | bytes 4196352 | tf_op jit(solution)/shard_map/jit(_take)/gather | solution.py:165
  29.7 3.3 gather_fusion
  33.0 1.5 fusion.23
  34.6 21.9 %all_to_all.15 = bf16[8,64,512]{2,1,0:T(8,128)(2,1)} all-to-all(bf16[8,64,512]{2,1,0:T(8,128)(2,1)S(1)} %get-tuple-element.222), channel_id=1, replica_groups=mesh['sp'=8,'tp'=4] {'sp'}, dimensions={0} | all-to-all | bytes 1048576 | tf_op jit(solution)/shard_map/all_to_all | solution.py:174
  56.5 17.6 %all_to_all.16 = bf16[8,64,512]{2,1,0:T(8,128)(2,1)} all-to-all(bf16[8,64,512]{2,1,0:T(8,128)(2,1)S(1)} %get-tuple-element.221), channel_id=1, replica_groups=mesh['sp'=8,'tp'=4] {'sp'}, dimensions={0} | all-to-all | bytes 1048576 | tf_op jit(solution)/shard_map/all_to_all | solution.py:175
  74.7 3.5 all-gather.8.cloned.1.call-done
  78.2 3.5 fusion.14
  81.7 1.5 fusion.20
  83.2 19.1 %all-gather.10.cloned.1.call-done = bf16[8,64,2048]{2,1,0:T(8,128)(2,1)} async-done(((bf16[8,64,512]{2,1,0:T(8,128)(2,1)}), bf16[8,64,2048]{2,1,0:T(8,128)(2,1)}) %all-gather.10.cloned.1.call-update) | async-done | bytes 2097168 | tf_op jit(solution)/shard_map/all_gather | solution.py:179
  102.3 3.1 select_convert_fusion
  106.9 2.1 add_convert_fusion
  109.2 0.8 fusion.47
  111.4 1.0 convolution_convert_fusion.4
  112.5 48.1 %all-reduce.3.cloned.1.call-done = bf16[8,64,2048]{2,1,0:T(8,128)(2,1)} async-done(((bf16[8,64,2048]{2,1,0:T(8,128)(2,1)}), bf16[8,64,2048]{2,1,0:T(8,128)(2,1)}) %all-reduce.3.cloned.1.call-update) | async-done | bytes 2097168 | tf_op jit(solution)/shard_map/psum | solution.py:186
  160.6 5.5 %all-to-all-start.2 = ((bf16[8,64,2048]{2,1,0:T(8,128)(2,1)}), bf16[8,64,2048]{2,1,0:T(8,128)(2,1)}, u32[]{:S(2)}, u32[]{:S(2)}) async-start(bf16[8,64,2048]{2,1,0:T(8,128)(2,1)} %all-reduce.3.cloned.1.call-done), calls=%async_computation.2 | async-start | bytes 4194304 | tf_op jit(solution)/shard_map/all_to_all | solution.py:187
  167.9 48.0 %all-reduce = bf16[16]{0:T(256)(128)(2,1)S(1)} all-reduce(bf16[16]{0:T(256)(128)(2,1)S(1)} %dynamic-update-slice), channel_id=3, replica_groups=mesh['sp'=8,'tp'=4] {'sp'}, use_global_device_ids=true, to_apply=%add | all-reduce | flops 16 | bytes 64
  219.1 1.1 multiply_reduce_fusion
  220.7 4.4 %gather_fusion.2 = bf16[256,2048]{1,0:T(8,128)(2,1)S(1)} fusion(bf16[512,2048]{1,0:T(8,128)(2,1)} %bitcast.19, s32[1024]{0:T(1024)} %pad_clamp_fusion), kind=kCustom, calls=%fused_computation.2 | custom fusion | bytes 2098176 | tf_op jit(solution)/shard_map/jit(_take)/gather | solution.py:196
  225.1 1.5 gather.23
  226.6 2.0 fusion.22
  228.8 1.6 fusion.62
  230.4 1.1 copy.169
  231.5 0.9 fusion.25
  232.4 1.1 fusion.26
  233.5 2.1 convolution_convert_fusion.3
  235.8 1.5 subtract_exponential_fusion
  238.0 1.2 fusion.29
  239.3 2.7 fusion.61
  242.0 0.8 copy-done.19
  243.5 3.5 fusion
  247.0 1.7 fusion.1
  249.2 1.8 fusion.2
  252.8 35.5 %all-gather.14.cloned.1.call-done = bf16[16,128,256]{2,1,0:T(8,128)(2,1)} async-done(((bf16[2,128,256]{2,1,0:T(8,128)(2,1)}), bf16[16,128,256]{2,1,0:T(8,128)(2,1)}) %all-gather.14.cloned.1.call-update) | async-done | bytes 1048592 | tf_op jit(solution)/shard_map/all_gather | solution.py:37
  288.4 12.1 %while.27 = (s32[]{:T(128)}, f32[2,128,256]{2,1,0:T(8,128)S(1)}, s32[]{:T(128)}, bf16[8,2,128,256]{3,2,1,0:T(8,128)(2,1)}, bf16[8,2]{1,0:T(8,128)(2,1)}, /*index=5*/s32[]{:T(128)}, s32[]{:T(128)}, s32[]{:T(128)}, s32[]{:T(128)}) while((s32[]{:T(128)}, f32[2,128,256]{2,1,0:T(8,128)S(1)}, s32[]{:T(128)}, bf16[8,2,128,256]{3,2,1,0:T(8,128)(2,1)}, ...), condition=%wide.region_12.13_spmd, body=%wide.region_11.12_spmd.sunk | while | flops 196616 | bytes 655535 | solution.py:54
  289.1 1.0 convert_add_fusion.5
  290.8 1.0 convert_add_fusion.5
  292.6 1.0 convert_add_fusion.5
  294.3 1.0 convert_add_fusion.5
  296.0 1.0 convert_add_fusion.5
  297.7 1.1 convert_add_fusion.5
  299.5 1.0 convert_add_fusion.5
  303.4 0.8 copy.181
  304.2 75.2 %reduce-scatter.2.cloned.1.call-done = f32[256,512]{1,0:T(8,128)} async-done(((f32[2048,512]{1,0:T(8,128)}), f32[256,512]{1,0:T(8,128)}) %reduce-scatter.2.cloned.1.call-update) | async-done | bytes 524304 | tf_op jit(solution)/shard_map/reduce_scatter | solution.py:245
  (180 shorter events, 22.9 us)
Async XLA Ops:
  8.0 220.8 %copy-start = (bf16[2048,512]{1,0:T(8,128)(2,1)S(1)}, bf16[2048,512]{1,0:T(8,128)(2,1)}, u32[]{:S(2)}) copy-start(bf16[2048,512]{1,0:T(8,128)(2,1)} %param.24) | copy-start | bytes 6291460
  8.0 70.2 %all-gather.8.cloned.1.call-start = ((), (), s32[]{:S(2)}) async-start(), calls=%async_computation.4 | async-start | bytes 2621440 | tf_op jit(solution)/shard_map/all_gather | solution.py:178
  16.1 3.7 copy-start.36
  23.0 6.7 %copy-start.1 = (bf16[128,2048]{1,0:T(8,128)(2,1)S(1)}, bf16[128,2048]{1,0:T(8,128)(2,1)}, u32[]{:S(2)}) copy-start(bf16[128,2048]{1,0:T(8,128)(2,1)} %param.16) | copy-start | bytes 1572868
  34.5 39.7 %copy-start.25 = (bf16[128,2,128]{2,1,0:T(2,128)(2,1)S(1)}, bf16[128,2,128]{2,1,0:T(2,128)(2,1)}, u32[]{:S(2)}) copy-start(bf16[128,2,128]{2,1,0:T(2,128)(2,1)} %param.20) | copy-start | bytes 196612
  34.6 39.9 %copy-start.26 = (bf16[128,2,128]{2,1,0:T(2,128)(2,1)S(1)}, bf16[128,2,128]{2,1,0:T(2,128)(2,1)}, u32[]{:S(2)}) copy-start(bf16[128,2,128]{2,1,0:T(2,128)(2,1)} %param.21) | copy-start | bytes 196612
  56.5 45.9 %all-gather.10.cloned.1.call-start = ((), (), s32[]{:S(2)}) async-start(), calls=%async_computation.5 | async-start | bytes 2621440 | tf_op jit(solution)/shard_map/all_gather | solution.py:179
  74.2 86.4 %all-reduce.3.cloned.1.call-start = ((), (), s32[]{:S(2)}) async-start(), calls=%async_computation.6 | async-start | bytes 4194304 | tf_op jit(solution)/shard_map/psum | solution.py:186
  74.4 7.3 %copy-start.14 = (bf16[1,2048,256]{2,1,0:T(8,128)(2,1)S(1)}, bf16[1,2048,256]{2,1,0:T(8,128)(2,1)}, u32[]{:S(2)}) copy-start(bf16[1,2048,256]{2,1,0:T(8,128)(2,1)} %param.25) | copy-start | bytes 3145732
  78.2 3.5 copy-start.38
  105.5 0.8 copy-start.20
  105.5 0.8 copy-start.22
  105.5 1.4 copy-start.15
  109.0 1.8 copy-start.37
  109.0 2.4 copy-start.6
  109.0 108.9 %all-gather.12.cloned.1.call-start = ((), (), s32[]{:S(2)}) async-start(), calls=%async_computation.8 | async-start | bytes 1179648 | tf_op jit(solution)/shard_map/all_gather | solution.py:15
  110.0 50.5 %copy-start.17 = (f32[128,64]{0,1:T(8,128)}, f32[128,64]{0,1:T(8,128)S(1)}, u32[]{:S(2)}) copy-start(f32[128,64]{0,1:T(8,128)S(1)} %get-tuple-element.216) | copy-start | bytes 98308
  110.6 50.0 %copy-start.8 = (f32[128,2,64,2]{0,3,2,1:T(2,128)}, f32[128,2,64,2]{0,3,2,1:T(2,128)S(1)}, u32[]{:S(2)}) copy-start(f32[128,2,64,2]{0,3,2,1:T(2,128)S(1)} %get-tuple-element.225) | copy-start | bytes 393220
  110.6 105.5 %copy-start.10 = (f32[128,2,64,2]{0,3,2,1:T(2,128)}, f32[128,2,64,2]{0,3,2,1:T(2,128)S(1)}, u32[]{:S(2)}) copy-start(f32[128,2,64,2]{0,3,2,1:T(2,128)S(1)} %get-tuple-element.224) | copy-start | bytes 393220
  111.0 49.5 %copy-start.16 = (f32[128,2]{1,0:T(8,128)}, f32[128,2]{1,0:T(8,128)S(1)}, u32[]{:S(2)}) copy-start(f32[128,2]{1,0:T(8,128)S(1)} %reduce_window_sum.28) | copy-start | bytes 3076
  111.1 106.4 %copy-start.27 = (f32[128,2]{0,1:T(2,128)}, f32[128,2]{0,1:T(2,128)S(1)}, u32[]{:S(2)}) copy-start(f32[128,2]{0,1:T(2,128)S(1)} %copy.162) | copy-start | bytes 3076
  111.3 49.3 %copy-start.34 = (f32[2]{0:T(128)}, f32[2]{0:T(128)S(1)}, u32[]{:S(2)}) copy-start(f32[2]{0:T(128)S(1)} %slice_reduce_fusion.1) | copy-start | bytes 28
  111.4 107.0 %copy-start.33 = (f32[2,128]{1,0:T(2,128)}, f32[2,128]{1,0:T(2,128)S(1)}, u32[]{:S(2)}) copy-start(f32[2,128]{1,0:T(2,128)S(1)} %get-tuple-element.219) | copy-start | bytes 3076
  112.4 53.7 %copy-start.41 = (u32[32]{0:T(128)S(1)}, u32[32]{0:T(128)}, u32[]{:S(2)}) copy-start(u32[32]{0:T(128)} %constant.181) | copy-start | bytes 388
  112.5 104.4 %copy-start.32 = (s32[128,2]{0,1:T(2,128)S(1)}, s32[128,2]{0,1:T(2,128)}, u32[]{:S(2)}) copy-start(s32[128,2]{0,1:T(2,128)} %param.18) | copy-start | bytes 3076
  160.6 60.1 %all-to-all-start.2 = ((bf16[8,64,2048]{2,1,0:T(8,128)(2,1)}), bf16[8,64,2048]{2,1,0:T(8,128)(2,1)}, u32[]{:S(2)}, u32[]{:S(2)}) async-start(bf16[8,64,2048]{2,1,0:T(8,128)(2,1)} %all-reduce.3.cloned.1.call-done), calls=%async_computation.2 | async-start | bytes 4194304 | tf_op jit(solution)/shard_map/all_to_all | solution.py:187
  166.1 122.2 %all-gather.14.cloned.1.call-start = ((), (), s32[]{:S(2)}) async-start(), calls=%async_computation.9 | async-start | bytes 1179648 | tf_op jit(solution)/shard_map/all_gather | solution.py:37
  216.2 2.1 copy-start.4
  218.0 2.7 copy-start.35
  226.6 2.0 copy-start.5
  228.8 2.7 copy-start.2
  235.6 143.8 %reduce-scatter.2.cloned.1.call-start = ((), (), s32[]{:S(2)}) async-start(), calls=%async_computation.7 | async-start | bytes 4718592 | tf_op jit(solution)/shard_map/reduce_scatter | solution.py:245
  242.0 0.8 copy-start.19
  242.0 1.5 copy-start.21
  243.5 3.5 copy-start.23
  243.5 3.5 copy-start.39
  247.0 1.8 copy-start.40
  247.0 1.8 copy-start.42
  247.0 2.2 copy-start.43
  249.2 1.8 copy-start.7
  249.2 1.8 copy-start.28
  249.2 2.1 copy-start.11
  249.2 2.4 copy-start.9
  249.2 2.8 copy-start.13
  249.2 3.2 copy-start.31
  252.4 48.1 %copy-start.29 = (f32[128,2]{0,1:T(2,128)S(1)}, f32[128,2]{0,1:T(2,128)}, u32[]{:S(2)}) copy-start(f32[128,2]{0,1:T(2,128)} %copy.174) | copy-start | bytes 3076
  288.4 12.5 %copy-start.18 = (f32[128,64]{0,1:T(8,128)S(1)}, f32[128,64]{0,1:T(8,128)}, u32[]{:S(2)}) copy-start(f32[128,64]{0,1:T(8,128)} %copy-done.17) | copy-start | bytes 98308
  288.4 12.5 %copy-start.24 = (f32[128,64]{0,1:T(8,128)S(1)}, f32[128,64]{0,1:T(8,128)}, u32[]{:S(2)}) copy-start(f32[128,64]{0,1:T(8,128)} %get-tuple-element.214) | copy-start | bytes 98308
  (3 other events, 2.0 us)
Sparse Core Ops, SparseCore 0:
  56.6 21.5 all-gather.7
  79.7 22.5 all-gather.9
  109.1 51.4 all-reduce.2
Sparse Core Ops, SparseCore 1:
  112.5 40.3 all-gather.11
  235.6 52.7 all-gather.13
  292.4 86.9 reduce-scatter.1
where the time goes:
time: 388 us; the launch traced here: 387 us
  waiting for transfers between devices  182 us (47%)
  blocking collectives  87.5 us (23%)
  local copies, waits for them, and re-layouts  35.9 us (9%)
  matrix products  29.6 us (8%)
  other arithmetic  29 us (7%)
  between operations  16.8 us (4%)
  starting transfers between devices  6.18 us (2%)
    reduce_scatter x1, waiting for transfers between devices, per_device(): lax.psum_scatter(lax.dot_general(resid_grad, normed_bf, (((0,), (0,)), ((...  75.2 us
    psum x1, waiting for transfers between devices, per_device(): summed = lax.psum(back_rows, 'tp').astype(jnp.float32).astype(jnp.bfloat16)  48.1 us
    unnamed x1, blocking collectives  48 us
    all_gather x1, waiting for transfers between devices, prefix_2(): lax.all_gather(a.astype(kind), axis)  35.5 us
    all_to_all x1, blocking collectives, per_device(): lax.all_to_all(quarters[0], 'sp', split_axis=0, concat_axis=0, tiled=True)  21.9 us
    all_gather x1, waiting for transfers between devices, per_device(): lax.all_gather(quarters[1], 'tp', axis=2, tiled=True)  19.1 us
    all_to_all x1, blocking collectives, per_device(): lax.all_to_all(quarters[1], 'sp', split_axis=0, concat_axis=0, tiled=True)  17.6 us
  transfers between devices with their start and end apart: 7, of which 5 were waited for; matrix products, arithmetic and copies ran while one was open for 11% of the time, Pallas kernels for 0%

commit v1 on v0

--- a/solution.py
+++ b/solution.py
@@ -183,7 +183,9 @@
     gate_part, up_part, down_part, back_rows = expert_local(
         routed_rows, routed_grads, gate_weight[0], up_weight[0], down_weight[0]
     )
-    summed = lax.psum(back_rows, "tp").astype(jnp.float32).astype(jnp.bfloat16)
+    summed = (
+        jnp.sum(lax.all_gather(back_rows, "tp"), axis=0).astype(jnp.float32).astype(jnp.bfloat16)
+    )
     returned = lax.all_to_all(
         summed.reshape(experts, capacity, model_width),
         "sp",

time: 388 us -> 412 us (1.062)
  blocking collectives: 87.5 us -> 97.4 us
  waiting for transfers between devices: 182 us -> 190 us
  other arithmetic: 29 us -> 35.6 us
    all_gather x0 -> x1, waiting for transfers between devices: none -> 53.9 us  [per_device(): lax.all_gather(back_rows, 'tp')]
    psum x1 -> x0, waiting for transfers between devices: 48.1 us -> none  [per_device(): summed = lax.psum(back_rows, 'tp').astype(jnp.float32).astype(jnp.bfloat16)]
    unnamed x1, blocking collectives: 48 us -> 58 us
    reduce_sum x0 -> x1, other arithmetic: none -> 7.18 us  [per_device(): jnp.sum(lax.all_gather(back_rows, 'tp'), axis=0).astype(jnp.float32)]
  transfers between devices with their start and end apart: 7 -> 7, of which waited for: 5 -> 5; matrix products, arithmetic and copies ran while one was open for 11% -> 12% of each run, Pallas kernels for 0% -> 0%
where the time goes in v1:
time: 412 us; the launch traced here: 411 us
  waiting for transfers between devices  190 us (46%)
  blocking collectives  97.4 us (24%)
  local copies, waits for them, and re-layouts  36.4 us (9%)
  other arithmetic  35.6 us (9%)
  matrix products  29.6 us (7%)
  between operations  15.5 us (4%)
  starting transfers between devices  6.3 us (2%)
    reduce_scatter x1, waiting for transfers between devices, per_device(): lax.psum_scatter(lax.dot_general(resid_grad, normed_bf, (((0,), (0,)), ((...  75.8 us
    unnamed x1, blocking collectives  58 us
    all_gather x1, waiting for transfers between devices, per_device(): lax.all_gather(back_rows, 'tp')  53.9 us
    all_gather x1, waiting for transfers between devices, prefix_2(): lax.all_gather(a.astype(kind), axis)  37.3 us
    all_to_all x1, blocking collectives, per_device(): lax.all_to_all(quarters[0], 'sp', split_axis=0, concat_axis=0, tiled=True)  21.7 us
    all_gather x1, waiting for transfers between devices, per_device(): lax.all_gather(quarters[1], 'tp', axis=2, tiled=True)  19.1 us
    all_to_all x1, blocking collectives, per_device(): lax.all_to_all(quarters[1], 'sp', split_axis=0, concat_axis=0, tiled=True)  17.6 us
    unnamed x99, local copies, waits for them, and re-layouts  8.28 us
  transfers between devices with their start and end apart: 7, of which 5 were waited for; matrix products, arithmetic and copies ran while one was open for 12% of the time, Pallas kernels for 0%

profile of v1, /device:TPU:0, one launch (start us, length us, event | category | flops | bytes accessed | tf_op | source)
XLA Modules:
  0.0 411.2 jit_solution(10300129677911326673)
XLA Ops:
  7.2 0.8 broadcast_multiply_fusion.1
  10.3 1.4 scatter_custom_fusion
  11.8 3.5 mul.382
  15.2 3.7 mul.383
  19.5 2.7 multiply_convert_fusion
  22.2 6.6 %gather_fusion.1 = bf16[512,2048]{1,0:T(8,128)(2,1)} fusion(bf16[256,2048]{1,0:T(8,128)(2,1)} %multiply_convert_fusion, s32[1024]{0:T(1024)S(1)} %pad_clamp_fusion.1), kind=kCustom, calls=%fused_computation.1 | custom fusion | bytes 4196352 | tf_op jit(solution)/shard_map/jit(_take)/gather | solution.py:165
  28.9 3.3 gather_fusion
  32.2 1.6 fusion.23
  33.7 21.7 %all_to_all.15 = bf16[8,64,512]{2,1,0:T(8,128)(2,1)} all-to-all(bf16[8,64,512]{2,1,0:T(8,128)(2,1)S(1)} %get-tuple-element.222), channel_id=1, replica_groups=mesh['sp'=8,'tp'=4] {'sp'}, dimensions={0} | all-to-all | bytes 1048576 | tf_op jit(solution)/shard_map/all_to_all | solution.py:174
  55.5 17.6 %all_to_all.16 = bf16[8,64,512]{2,1,0:T(8,128)(2,1)} all-to-all(bf16[8,64,512]{2,1,0:T(8,128)(2,1)S(1)} %get-tuple-element.221), channel_id=1, replica_groups=mesh['sp'=8,'tp'=4] {'sp'}, dimensions={0} | all-to-all | bytes 1048576 | tf_op jit(solution)/shard_map/all_to_all | solution.py:175
  73.2 4.0 all-gather.10.cloned.1.call-done
  77.2 3.5 fusion.14
  80.7 1.5 fusion.20
  82.2 19.1 %all-gather.12.cloned.1.call-done = bf16[8,64,2048]{2,1,0:T(8,128)(2,1)} async-done(((bf16[8,64,512]{2,1,0:T(8,128)(2,1)}), bf16[8,64,2048]{2,1,0:T(8,128)(2,1)}) %all-gather.12.cloned.1.call-update) | async-done | bytes 2097168 | tf_op jit(solution)/shard_map/all_gather | solution.py:179
  101.4 3.1 select_convert_fusion
  105.9 2.0 add_convert_fusion
  109.3 0.8 fusion.47
  111.4 1.1 convolution_convert_fusion.4
  112.5 53.9 %all-gather.14.cloned.1.call-done = bf16[2048,2048]{1,0:T(8,128)(2,1)} async-done(((bf16[512,2048]{1,0:T(8,128)(2,1)}), bf16[2048,2048]{1,0:T(8,128)(2,1)}) %all-gather.14.cloned.1.call-update) | async-done | bytes 8388624 | tf_op jit(solution)/shard_map/all_gather | solution.py:187
  166.4 7.2 %reduce_sum.46 = bf16[512,2048]{1,0:T(8,128)(2,1)} reduce(bf16[4,512,2048]{2,1,0:T(8,128)(2,1)} %bitcast.180, bf16[]{:T(256)} %constant.154.clone.1), dimensions={0}, to_apply=%region_4.5 | reduce | flops 3145728 | bytes 10485762 | tf_op jit(solution)/shard_map/reduce_sum | solution.py:187
  173.7 5.7 %all-to-all-start.2 = ((bf16[8,64,2048]{2,1,0:T(8,128)(2,1)}), bf16[8,64,2048]{2,1,0:T(8,128)(2,1)}, u32[]{:S(2)}, u32[]{:S(2)}) async-start(bf16[8,64,2048]{2,1,0:T(8,128)(2,1)} %bitcast.181), calls=%async_computation.2 | async-start | bytes 4194304 | tf_op jit(solution)/shard_map/all_to_all | solution.py:189
  181.1 58.0 %all-reduce = bf16[16]{0:T(256)(128)(2,1)S(1)} all-reduce(bf16[16]{0:T(256)(128)(2,1)S(1)} %dynamic-update-slice), channel_id=4, replica_groups=mesh['sp'=8,'tp'=4] {'sp'}, use_global_device_ids=true, to_apply=%add | all-reduce | flops 16 | bytes 64
  242.2 1.1 multiply_reduce_fusion
  243.9 4.4 %gather_fusion.2 = bf16[256,2048]{1,0:T(8,128)(2,1)S(1)} fusion(bf16[512,2048]{1,0:T(8,128)(2,1)} %bitcast.20, s32[1024]{0:T(1024)} %pad_clamp_fusion), kind=kCustom, calls=%fused_computation.2 | custom fusion | bytes 2098176 | tf_op jit(solution)/shard_map/jit(_take)/gather | solution.py:198
  248.2 1.5 gather.23
  249.7 2.0 fusion.22
  251.9 1.6 fusion.62
  253.5 1.1 copy.169
  254.6 0.9 fusion.25
  255.5 1.1 fusion.26
  256.6 2.0 convolution_convert_fusion.3
  259.0 1.5 subtract_exponential_fusion
  261.1 1.2 fusion.29
  262.4 2.7 fusion.61
  265.1 0.8 copy-done.19
  266.6 3.5 fusion
  270.1 1.7 fusion.1
  272.3 1.8 fusion.2
  275.9 37.3 %all-gather.18.cloned.1.call-done = bf16[16,128,256]{2,1,0:T(8,128)(2,1)} async-done(((bf16[2,128,256]{2,1,0:T(8,128)(2,1)}), bf16[16,128,256]{2,1,0:T(8,128)(2,1)}) %all-gather.18.cloned.1.call-update) | async-done | bytes 1048592 | tf_op jit(solution)/shard_map/all_gather | solution.py:37
  313.3 11.7 %while.27 = (s32[]{:T(128)}, f32[2,128,256]{2,1,0:T(8,128)S(1)}, s32[]{:T(128)}, bf16[8,2,128,256]{3,2,1,0:T(8,128)(2,1)}, bf16[8,2]{1,0:T(8,128)(2,1)}, /*index=5*/s32[]{:T(128)}, s32[]{:T(128)}, s32[]{:T(128)}, s32[]{:T(128)}) while((s32[]{:T(128)}, f32[2,128,256]{2,1,0:T(8,128)S(1)}, s32[]{:T(128)}, bf16[8,2,128,256]{3,2,1,0:T(8,128)(2,1)}, ...), condition=%wide.region_12.13_spmd, body=%wide.region_11.12_spmd.sunk | while | flops 196616 | bytes 655535 | solution.py:54
  313.9 1.0 convert_add_fusion.5
  315.6 1.0 convert_add_fusion.5
  317.2 1.0 convert_add_fusion.5
  318.9 1.0 convert_add_fusion.5
  320.6 1.0 convert_add_fusion.5
  322.2 1.0 convert_add_fusion.5
  323.9 1.0 convert_add_fusion.5
  328.6 75.8 %reduce-scatter.2.cloned.1.call-done = f32[256,512]{1,0:T(8,128)} async-done(((f32[2048,512]{1,0:T(8,128)}), f32[256,512]{1,0:T(8,128)}) %reduce-scatter.2.cloned.1.call-update) | async-done | bytes 524304 | tf_op jit(solution)/shard_map/reduce_scatter | solution.py:247
  (181 shorter events, 23.7 us)
Async XLA Ops:
  7.2 244.7 %copy-start = (bf16[2048,512]{1,0:T(8,128)(2,1)S(1)}, bf16[2048,512]{1,0:T(8,128)(2,1)}, u32[]{:S(2)}) copy-start(bf16[2048,512]{1,0:T(8,128)(2,1)} %param.24) | copy-start | bytes 6291460
  7.2 70.0 %all-gather.10.cloned.1.call-start = ((), (), s32[]{:S(2)}) async-start(), calls=%async_computation.4 | async-start | bytes 2621440 | tf_op jit(solution)/shard_map/all_gather | solution.py:178
  15.2 3.7 copy-start.36
  22.2 6.7 %copy-start.1 = (bf16[128,2048]{1,0:T(8,128)(2,1)S(1)}, bf16[128,2048]{1,0:T(8,128)(2,1)}, u32[]{:S(2)}) copy-start(bf16[128,2048]{1,0:T(8,128)(2,1)} %param.16) | copy-start | bytes 1572868
  55.5 45.9 %all-gather.12.cloned.1.call-start = ((), (), s32[]{:S(2)}) async-start(), calls=%async_computation.5 | async-start | bytes 2621440 | tf_op jit(solution)/shard_map/all_gather | solution.py:179
  73.2 7.6 %copy-start.14 = (bf16[1,2048,256]{2,1,0:T(8,128)(2,1)S(1)}, bf16[1,2048,256]{2,1,0:T(8,128)(2,1)}, u32[]{:S(2)}) copy-start(bf16[1,2048,256]{2,1,0:T(8,128)(2,1)} %param.25) | copy-start | bytes 3145732
  73.2 93.3 %all-gather.14.cloned.1.call-start = ((), (), s32[]{:S(2)}) async-start(), calls=%async_computation.7 | async-start | bytes 10485760 | tf_op jit(solution)/shard_map/all_gather | solution.py:187
  77.2 3.5 copy-start.38
  104.5 0.8 copy-start.20
  104.5 0.8 copy-start.22
  104.5 1.4 copy-start.15
  108.0 0.8 copy-start.25
  108.0 1.0 copy-start.26
  108.0 2.8 copy-start.37
  108.0 3.5 copy-start.6
  108.0 133.1 %all-gather.16.cloned.1.call-start = ((), (), s32[]{:S(2)}) async-start(), calls=%async_computation.8 | async-start | bytes 1179648 | tf_op jit(solution)/shard_map/all_gather | solution.py:15
  110.7 63.0 %copy-start.8 = (f32[128,2,64,2]{0,3,2,1:T(2,128)}, f32[128,2,64,2]{0,3,2,1:T(2,128)S(1)}, u32[]{:S(2)}) copy-start(f32[128,2,64,2]{0,3,2,1:T(2,128)S(1)} %get-tuple-element.225) | copy-start | bytes 393220
  110.7 128.7 %copy-start.10 = (f32[128,2,64,2]{0,3,2,1:T(2,128)}, f32[128,2,64,2]{0,3,2,1:T(2,128)S(1)}, u32[]{:S(2)}) copy-start(f32[128,2,64,2]{0,3,2,1:T(2,128)S(1)} %get-tuple-element.224) | copy-start | bytes 393220
  111.1 62.5 %copy-start.16 = (f32[128,2]{1,0:T(8,128)}, f32[128,2]{1,0:T(8,128)S(1)}, u32[]{:S(2)}) copy-start(f32[128,2]{1,0:T(8,128)S(1)} %reduce_window_sum.28) | copy-start | bytes 3076
  111.1 129.5 %copy-start.27 = (f32[128,2]{0,1:T(2,128)}, f32[128,2]{0,1:T(2,128)S(1)}, u32[]{:S(2)}) copy-start(f32[128,2]{0,1:T(2,128)S(1)} %copy.162) | copy-start | bytes 3076
  111.3 62.3 %copy-start.34 = (f32[2]{0:T(128)}, f32[2]{0:T(128)S(1)}, u32[]{:S(2)}) copy-start(f32[2]{0:T(128)S(1)} %slice_reduce_fusion.1) | copy-start | bytes 28
  111.4 130.1 %copy-start.33 = (f32[2,128]{1,0:T(2,128)}, f32[2,128]{1,0:T(2,128)S(1)}, u32[]{:S(2)}) copy-start(f32[2,128]{1,0:T(2,128)S(1)} %get-tuple-element.219) | copy-start | bytes 3076
  173.6 5.7 %copy-start.41 = (u32[32]{0:T(128)S(1)}, u32[32]{0:T(128)}, u32[]{:S(2)}) copy-start(u32[32]{0:T(128)} %constant.182) | copy-start | bytes 388
  173.6 66.5 %copy-start.32 = (s32[128,2]{0,1:T(2,128)S(1)}, s32[128,2]{0,1:T(2,128)}, u32[]{:S(2)}) copy-start(s32[128,2]{0,1:T(2,128)} %param.18) | copy-start | bytes 3076
  173.7 70.2 %all-to-all-start.2 = ((bf16[8,64,2048]{2,1,0:T(8,128)(2,1)}), bf16[8,64,2048]{2,1,0:T(8,128)(2,1)}, u32[]{:S(2)}, u32[]{:S(2)}) async-start(bf16[8,64,2048]{2,1,0:T(8,128)(2,1)} %bitcast.181), calls=%async_computation.2 | async-start | bytes 4194304 | tf_op jit(solution)/shard_map/all_to_all | solution.py:189
  179.3 133.9 %all-gather.18.cloned.1.call-start = ((), (), s32[]{:S(2)}) async-start(), calls=%async_computation.9 | async-start | bytes 1179648 | tf_op jit(solution)/shard_map/all_gather | solution.py:37
  239.5 2.0 copy-start.4
  241.1 2.7 copy-start.35
  241.5 0.7 copy-start.3
  249.7 2.0 copy-start.5
  251.9 2.7 copy-start.2
  258.7 145.7 %reduce-scatter.2.cloned.1.call-start = ((), (), s32[]{:S(2)}) async-start(), calls=%async_computation.6 | async-start | bytes 4718592 | tf_op jit(solution)/shard_map/reduce_scatter | solution.py:247
  265.1 0.8 copy-start.19
  265.1 1.5 copy-start.21
  266.6 3.5 copy-start.23
  266.6 3.5 copy-start.39
  270.0 1.8 copy-start.40
  270.0 1.8 copy-start.42
  270.0 2.2 copy-start.43
  272.2 1.8 copy-start.7
  272.2 1.8 copy-start.28
  272.2 2.1 copy-start.11
  272.3 2.4 copy-start.9
  272.3 2.8 copy-start.13
  272.3 3.2 copy-start.31
  275.5 49.4 %copy-start.29 = (f32[128,2]{0,1:T(2,128)S(1)}, f32[128,2]{0,1:T(2,128)}, u32[]{:S(2)}) copy-start(f32[128,2]{0,1:T(2,128)} %copy.174) | copy-start | bytes 3076
  313.2 12.0 %copy-start.18 = (f32[128,64]{0,1:T(8,128)S(1)}, f32[128,64]{0,1:T(8,128)}, u32[]{:S(2)}) copy-start(f32[128,64]{0,1:T(8,128)} %copy-done.17) | copy-start | bytes 98308
  313.2 12.0 %copy-start.24 = (f32[128,64]{0,1:T(8,128)S(1)}, f32[128,64]{0,1:T(8,128)}, u32[]{:S(2)}) copy-start(f32[128,64]{0,1:T(8,128)} %get-tuple-element.214) | copy-start | bytes 98308
  (3 other events, 1.9 us)
Sparse Core Ops, SparseCore 0:
  55.6 21.5 all-gather.9
  78.8 22.5 all-gather.11
  108.1 58.2 all-gather.13
  169.0 64.6 all-gather.15
  258.8 54.3 all-gather.17
  317.3 87.0 reduce-scatter.1
